TPU v7x, 32 devices: a whole 2x2x4 slice. The times are simulated.
32 devices in a mesh: sp: 16 (over z, x, core), tp: 2 (over y).
Axes of the slice: x: 2, y: 2, z: 4, core: 2. Of those that a mesh axis runs over, the one named last changes fastest.
Arguments:
- moe_input: bfloat16 [4096, 2048], P('sp'), may hold values from -6 to 6
- out_grad: bfloat16 [4096, 2048], P('sp'), may hold values from -0.29882812 to 0.29882812
- route_ids: int32 [4096, 2], P('sp'), may hold values from 0 to 15, all different within a row; in each aligned block of 256 rows (0 to 255, 256 to 511, ...) at most 40 rows name the same one
- route_weights: float32 [4096, 2], P('sp'), may hold values from 0.2 to 1
- gate_weight: bfloat16 [16, 1024, 2048], P('sp', 'tp'), may hold values from -0.1875 to 0.1875
- lin_weight: bfloat16 [16, 1024, 2048], P('sp', 'tp'), may hold values from -0.1875 to 0.1875
- down_weight: bfloat16 [16, 1024, 2048], P('sp', 'tp'), may hold values from -0.1875 to 0.1875
- outer_gate: bfloat16 [4096, 2048], P('sp', 'tp'), may hold values from -6 to 6
- inner_gate: bfloat16 [4096, 2048], P('sp', 'tp'), may hold values from -6 to 6
- conv_input: bfloat16 [4096, 2048], P('sp', 'tp'), may hold values from -6 to 6
- conv_taps: float32 [3, 2048], P(None, 'tp'), may hold values from -3.5 to 3.5
- out_proj: bfloat16 [2048, 2048], P('tp', 'sp'), may hold values from -0.125 to 0.125
Outputs:
- gate_weight_grad: bfloat16 [16, 1024, 2048], P('sp', 'tp')
- lin_weight_grad: bfloat16 [16, 1024, 2048], P('sp', 'tp')
- down_weight_grad: bfloat16 [16, 1024, 2048], P('sp', 'tp')
- out_proj_grad: float32 [2048, 2048], P('sp', 'tp')
- outer_gate_grad: bfloat16 [4096, 2048], P('sp', 'tp')
- inner_gate_grad: bfloat16 [4096, 2048], P('sp', 'tp')
- conv_input_grad: bfloat16 [4096, 2048], P('sp', 'tp')
Inputs may be any that keep to these rules, and one draw needn't show every extreme that they name: `route_ids`: each row names 2 different experts. Among the rows of one device no expert is named more than 40 times, a bound that some block reaches.
All inputs are finite; a program needn't handle non-finite values.
Results may differ from a plain program's by a relative error of at most 0.015.
Values may be sent and summed in bfloat16 or wider, within the bound.
A program may use at most 64 MiB of HBM per device.

v0:
```python
import jax
import jax.numpy as jnp
from jax import lax
from jax.sharding import PartitionSpec as P

LIMIT = 7.0
ALPHA = 1.702


def from_behind(value, axis, by):
    count = lax.axis_size(axis)
    pairs = [(i, i + by) for i in range(count) if 0 <= i + by < count]
    return lax.ppermute(value, axis, pairs)


def slot_layout(flat_ids, experts, capacity):
    onehot = (flat_ids[:, None] == jnp.arange(experts, dtype=jnp.int32)[None, :]).astype(jnp.int32)
    before = jnp.cumsum(onehot, axis=0) - onehot
    slot_rank = jnp.sum(before * onehot, axis=1)
    position = flat_ids * capacity + slot_rank
    pair_index = jnp.arange(flat_ids.shape[0], dtype=jnp.int32)
    source = jnp.full((experts * capacity,), -1, jnp.int32).at[position].set(pair_index)
    return (position, source)


def expert_terms(routed, cotan, gate_w, lin_w, down_w):
    gate_pre = jnp.einsum("xfd,xrd->xfr", gate_w, routed, preferred_element_type=jnp.float32)
    lin_pre = jnp.einsum("xfd,xrd->xfr", lin_w, routed, preferred_element_type=jnp.float32)
    gate_cut = jnp.minimum(gate_pre, LIMIT)
    lin_cut = jnp.clip(lin_pre, -LIMIT, LIMIT)
    sigma = jax.nn.sigmoid(ALPHA * gate_cut)
    act = (gate_cut * sigma * (lin_cut + 1.0)).astype(jnp.bfloat16)
    act_grad = jnp.einsum("xfd,xrd->xfr", down_w, cotan, preferred_element_type=jnp.float32)
    down_grad = jnp.einsum("xfr,xrd->xfd", act, cotan, preferred_element_type=jnp.float32)
    slope = sigma * (1.0 + ALPHA * gate_cut * (1.0 - sigma))
    gate_cot = jnp.where(gate_pre < LIMIT, act_grad * (lin_cut + 1.0) * slope, 0.0).astype(
        jnp.bfloat16
    )
    lin_cot = jnp.where(jnp.abs(lin_pre) < LIMIT, act_grad * gate_cut * sigma, 0.0).astype(
        jnp.bfloat16
    )
    gate_grad = jnp.einsum("xfr,xrd->xfd", gate_cot, routed, preferred_element_type=jnp.float32)
    lin_grad = jnp.einsum("xfr,xrd->xfd", lin_cot, routed, preferred_element_type=jnp.float32)
    input_part = jnp.einsum("xfr,xfd->xrd", gate_cot, gate_w, preferred_element_type=jnp.float32)
    input_part = input_part + jnp.einsum(
        "xfr,xfd->xrd", lin_cot, lin_w, preferred_element_type=jnp.float32
    )
    return (gate_grad, lin_grad, down_grad, input_part.astype(jnp.bfloat16))


def local(
    moe_input,
    out_grad,
    route_ids,
    route_weights,
    gate_weight,
    lin_weight,
    down_weight,
    outer_gate,
    inner_gate,
    conv_input,
    conv_taps,
    out_proj,
):
    sp_count = lax.axis_size("sp")
    tp_count = lax.axis_size("tp")
    local_experts = gate_weight.shape[0]
    experts = local_experts * sp_count
    tokens, top_count = route_ids.shape
    width = moe_input.shape[1]
    width_dev = width // tp_count
    capacity = 5 * tokens // (2 * experts)
    position, source = slot_layout(route_ids.reshape(-1), experts, capacity)
    filled = source >= 0
    picked = jnp.maximum(source, 0)
    token_row = picked // top_count
    send_rows = jnp.where(filled[:, None], moe_input[token_row], jnp.zeros((), jnp.bfloat16))
    send_rows = send_rows.reshape(experts, capacity, width)
    slot_weight = jnp.where(filled, route_weights.reshape(-1)[picked], 0.0)
    send_grads = (
        (slot_weight[:, None] * out_grad[token_row])
        .astype(jnp.bfloat16)
        .reshape(experts, capacity, width)
    )
    column_start = lax.axis_index("tp") * width_dev
    part_rows = lax.dynamic_slice_in_dim(send_rows, column_start, width_dev, 2)
    part_grads = lax.dynamic_slice_in_dim(send_grads, column_start, width_dev, 2)
    routed_part, cotan_part = (
        lax.all_to_all(part_rows, "sp", split_axis=0, concat_axis=1, tiled=True),
        lax.all_to_all(part_grads, "sp", split_axis=0, concat_axis=1, tiled=True),
    )
    routed, cotan = (
        lax.all_gather(routed_part, "tp", axis=2, tiled=True),
        lax.all_gather(cotan_part, "tp", axis=2, tiled=True),
    )
    expert_out = expert_terms(routed, cotan, gate_weight, lin_weight, down_weight)
    totals = expert_out[:3]
    input_part = expert_out[3]
    slot_count = input_part.shape[1]
    exchanged = lax.all_to_all(
        input_part.reshape(local_experts * slot_count, tp_count, width_dev),
        "tp",
        split_axis=1,
        concat_axis=1,
        tiled=True,
    )
    slot_sums = jnp.sum(exchanged.astype(jnp.float32), axis=1).astype(jnp.bfloat16)
    slot_sums = slot_sums.reshape(local_experts, slot_count, width_dev)
    returned = lax.all_to_all(slot_sums, "sp", split_axis=1, concat_axis=0, tiled=True)
    pair_grads = returned.reshape(experts * capacity, width_dev)[position].astype(jnp.float32)
    row_grads = jnp.sum(pair_grads.reshape(tokens, top_count, width_dev), axis=1).astype(
        jnp.bfloat16
    )
    full_rows = lax.all_gather(row_grads, "tp", axis=1, tiled=True)
    stream_grad = (out_grad.astype(jnp.float32) + full_rows.astype(jnp.float32)).astype(
        jnp.bfloat16
    )
    tap_count = conv_taps.shape[0]
    conv_values = (inner_gate.astype(jnp.float32) * conv_input.astype(jnp.float32)).astype(
        jnp.bfloat16
    )
    prior_rows = from_behind(conv_values[tokens - (tap_count - 1) :], "sp", 1)
    extended = jnp.concatenate([prior_rows, conv_values], axis=0).astype(jnp.float32)
    convolved = jnp.zeros((tokens, width_dev), jnp.float32)
    for tap_index in range(tap_count):
        convolved = (
            convolved + conv_taps[tap_index][None, :] * extended[tap_index : tap_index + tokens]
        )
    mixed = (outer_gate.astype(jnp.float32) * convolved).astype(jnp.bfloat16)
    columns = stream_grad
    mixed_grad = lax.dot_general(
        columns,
        lax.all_gather(out_proj, "sp", axis=1, tiled=True),
        (((1,), (1,)), ((), ())),
        preferred_element_type=jnp.float32,
    )
    columns = stream_grad
    out_proj_grad = lax.psum_scatter(
        lax.dot_general(
            columns, mixed, (((0,), (0,)), ((), ())), preferred_element_type=jnp.float32
        ),
        "sp",
        scatter_dimension=0,
        tiled=True,
    )
    outer_gate_grad = (mixed_grad * convolved).astype(jnp.bfloat16)
    conv_cot = (mixed_grad * outer_gate.astype(jnp.float32)).astype(jnp.bfloat16)
    later_rows = from_behind(conv_cot[: tap_count - 1], "sp", -1)
    extended_cot = jnp.concatenate([conv_cot, later_rows], axis=0).astype(jnp.float32)
    value_grad = jnp.zeros((tokens, width_dev), jnp.float32)
    for tap_index in range(tap_count):
        first_row = tap_count - 1 - tap_index
        value_grad = (
            value_grad
            + conv_taps[tap_index][None, :] * extended_cot[first_row : first_row + tokens]
        )
    inner_gate_grad = (value_grad * conv_input.astype(jnp.float32)).astype(jnp.bfloat16)
    conv_input_grad = (value_grad * inner_gate.astype(jnp.float32)).astype(jnp.bfloat16)
    return (
        totals[0].astype(jnp.bfloat16),
        totals[1].astype(jnp.bfloat16),
        totals[2].astype(jnp.bfloat16),
        out_proj_grad,
        outer_gate_grad,
        inner_gate_grad,
        conv_input_grad,
    )


def solution(mesh):
    placed = (
        P("sp", None),
        P("sp", None),
        P("sp", None),
        P("sp", None),
        P("sp", "tp", None),
        P("sp", "tp", None),
        P("sp", "tp", None),
        P("sp", "tp"),
        P("sp", "tp"),
        P("sp", "tp"),
        P(None, "tp"),
        P("tp", "sp"),
    )
    return jax.shard_map(
        local,
        mesh=mesh,
        in_specs=placed,
        out_specs=(
            P("sp", "tp", None),
            P("sp", "tp", None),
            P("sp", "tp", None),
            P("sp", "tp"),
            P("sp", "tp"),
            P("sp", "tp"),
            P("sp", "tp"),
        ),
        check_vma=False,
    )
```

profile of v0, /device:TPU:0, one launch (start us, length us, event | category | flops | bytes accessed | tf_op | source)
XLA Modules:
  0.0 397.4 jit_solution(9651991339992884759)
XLA Ops:
  7.2 0.8 broadcast_multiply_fusion
  8.0 0.8 copy.31
  9.4 1.2 reduce-window.6
  11.0 2.4 scatter_custom_fusion
  13.4 0.8 copy.34
  14.4 4.3 %gather_fusion.1 = f32[640]{0:T(1024)S(1)} fusion(f32[512]{0:T(512)S(1)} %reshape.176, s32[1024]{0:T(1024)S(1)} %get-tuple-element.21), kind=kCustom, calls=%fused_computation.1 | custom fusion | bytes 7680 | tf_op jit(solution)/shard_map/gather | solution.py:79
  18.9 4.1 %gather_fusion = bf16[640,2048]{1,0:T(8,128)(2,1)} fusion(bf16[256,2048]{1,0:T(8,128)(2,1)S(1)} %copy-done.3, s32[1024]{0:T(1024)S(1)} %get-tuple-element.22), kind=kCustom, calls=%fused_computation | custom fusion | bytes 5245440 | tf_op jit(solution)/shard_map/gather | solution.py:77
  22.9 2.8 dynamic-slice_select_fusion
  25.7 7.4 %all-to-all-start = ((bf16[16,40,1024]{2,1,0:T(8,128)(2,1)}), bf16[16,40,1024]{2,1,0:T(8,128)(2,1)}, u32[]{:S(2)}, u32[]{:S(2)}) async-start(bf16[16,40,1024]{2,1,0:T(8,128)(2,1)} %dynamic-slice_select_fusion), calls=%async_computation | async-start | bytes 2621440 | tf_op jit(solution)/shard_map/all_to_all | solution.py:89
  33.3 4.1 %gather_fusion.2 = bf16[640,2048]{1,0:T(8,128)(2,1)} fusion(bf16[256,2048]{1,0:T(8,128)(2,1)S(1)} %copy-done.2, s32[1024]{0:T(1024)S(1)} %get-tuple-element.22), kind=kCustom, calls=%fused_computation.2 | custom fusion | bytes 5245440 | tf_op jit(solution)/shard_map/gather | solution.py:81
  37.4 23.1 %all-to-all-done = bf16[16,40,1024]{2,1,0:T(8,128)(2,1)} async-done(((bf16[16,40,1024]{2,1,0:T(8,128)(2,1)}), bf16[16,40,1024]{2,1,0:T(8,128)(2,1)}, u32[]{:S(2)}, u32[]{:S(2)}) %all-to-all-start) | async-done | bytes 1310752 | tf_op jit(solution)/shard_map/all_to_all | solution.py:89
  60.6 1.6 fusion.3
  62.2 39.3 %all_to_all.38 = bf16[16,40,1024]{2,1,0:T(8,128)(2,1)} all-to-all(bf16[16,40,1024]{2,1,0:T(8,128)(2,1)S(1)} %fusion.3), channel_id=1, replica_groups=mesh['sp'=16,'tp'=2] {'sp'}, dimensions={0} | all-to-all | bytes 2621440 | tf_op jit(solution)/shard_map/all_to_all | solution.py:90
  101.7 0.5 all-gather.11.cloned.1.call-update
  102.2 0.9 all-gather.5.cloned.1.call-done
  103.1 5.1 %fusion.9 = f32[640,512]{1,0:T(8,128)} fusion(bf16[1,640,2048]{2,1,0:T(8,128)(2,1)} %all-gather.5.cloned.1.call-done, bf16[1,512,2048]{2,1,0:T(8,128)(2,1)} %param.17), kind=kOutput, calls=%fused_computation.20 | convolution fusion | flops 1342177280 | bytes 6029312 | tf_op jit(solution)/shard_map/xfd,xrd->xfr/dot_general | solution.py:28
  108.2 2.6 fusion.11
  110.8 32.8 %all-gather.7.cloned.1.call-done = bf16[1,640,2048]{2,1,0:T(8,128)(2,1)} async-done(((bf16[1,640,1024]{2,1,0:T(8,128)(2,1)}), bf16[1,640,2048]{2,1,0:T(8,128)(2,1)}) %all-gather.7.cloned.1.call-update) | async-done | bytes 2621456 | tf_op jit(solution)/shard_map/all_gather | solution.py:94
  143.6 5.4 %fusion.26 = (bf16[512,640]{0,1:T(8,128)(2,1)S(1)}, bf16[512,640]{0,1:T(8,128)(2,1)S(1)}) fusion(f32[640,512]{1,0:T(8,128)} %fusion.9, f32[640,512]{1,0:T(8,128)} %fusion.11, bf16[1,512,2048]{2,1,0:T(8,128)(2,1)} %param.18, bf16[1,640,2048]{2,1,0:T(8,128)(2,1)} %all-gather.7.cloned.1.call-done), kind=kOutput, calls=%fused_computation.44 | convolution fusion | flops 1349386240 | bytes 8650752 | tf_op jit(solution)/shard_map/xfd,xrd->xfr/dot_general | solution.py:33
  149.1 1.6 fusion.16
  151.1 1.5 add_convert_fusion
  152.9 34.3 %all_to_all.39 = bf16[640,2,1024]{2,0,1:T(8,128)(2,1)} all-to-all(bf16[640,2,1024]{2,0,1:T(8,128)(2,1)S(1)} %bitcast.131), channel_id=1, replica_groups=mesh['sp'=16,'tp'=2] {'tp'}, dimensions={1} | all-to-all | bytes 5242880 | tf_op jit(solution)/shard_map/all_to_all | solution.py:100
  187.2 2.7 reduce_sum.37
  189.9 3.5 copy.46
  193.5 0.5 broadcast.156
  194.0 9.6 %reduce.4 = bf16[640,1024]{1,0:T(8,128)(2,1)S(1)} reduce(bf16[640,1,1024]{2,1,0:T(2,128)(2,1)} %bitcast.132, bf16[]{:T(256)} %broadcast.156), dimensions={1}, to_apply=%bitcast.129.reduce_sub_computation | reduce | bytes 2621442
  203.6 1.7 reshape.230
  205.3 5.6 %all-to-all-start.3 = ((bf16[16,2,20480]{2,1,0:T(2,128)(2,1)}), bf16[16,2,20480]{2,1,0:T(2,128)(2,1)S(1)}, u32[]{:S(2)}, u32[]{:S(2)}) async-start(bf16[16,2,20480]{2,1,0:T(2,128)(2,1)} %reshape.230), calls=%async_computation.3 | async-start | bytes 2621440 | tf_op jit(solution)/shard_map/all_to_all | solution.py:109
  211.2 27.0 %all-to-all-done.3 = bf16[16,2,20480]{2,1,0:T(2,128)(2,1)S(1)} async-done(((bf16[16,2,20480]{2,1,0:T(2,128)(2,1)}), bf16[16,2,20480]{2,1,0:T(2,128)(2,1)S(1)}, u32[]{:S(2)}, u32[]{:S(2)}) %all-to-all-start.3) | async-done | bytes 1310752 | tf_op jit(solution)/shard_map/all_to_all | solution.py:109
  238.2 3.7 reshape.231
  241.9 2.2 copy.45
  244.1 2.8 gather_fusion.3
  246.9 1.6 gather.21
  248.4 3.6 reduce_sum.38
  252.3 2.9 collective-permute-start
  255.2 0.8 collective-permute-done
  256.0 1.1 maximum_convert_fusion
  257.2 18.8 %all-gather.9.cloned.1.call-done = bf16[256,2048]{1,0:T(8,128)(2,1)} async-done(((bf16[256,1024]{1,0:T(8,128)(2,1)}), bf16[256,2048]{1,0:T(8,128)(2,1)}) %all-gather.9.cloned.1.call-update) | async-done | bytes 1048592 | tf_op jit(solution)/shard_map/all_gather | solution.py:114
  275.9 6.2 %multiply_convert_fusion = (bf16[256,1024]{1,0:T(8,128)(2,1)}, f32[256,1024]{1,0:T(8,128)S(1)}, bf16[256,1024]{1,0:T(8,128)(2,1)}) fusion(f32[258,1024]{1,0:T(8,128)} %maximum_convert_fusion, f32[1024]{0:T(1024)S(1)} %bitcast.141, f32[1024]{0:T(1024)S(1)} %bitcast.143, f32[1024]{0:T(1024)S(1)} %bitcast.139, bf16[256,1024]{1,0:T(8,128)(2,1)} %param.19, ...), kind=kOutput, calls=%fused_computation.70 | convolution fusion | flops 1078460416 | bytes 12070912 | tf_op jit(solution)/shard_map/dot_general | solution.py:131
  282.1 4.6 %fusion.48 = f32[2048,1024]{1,0:T(8,128)} fusion(f32[256,1024]{1,0:T(8,128)S(1)} %get-tuple-element.10, bf16[256,1024]{1,0:T(8,128)(2,1)S(1)} %copy-done.15, bf16[256,2048]{1,0:T(8,128)(2,1)S(1)} %copy-done.11, bf16[256,2048]{1,0:T(8,128)(2,1)S(1)} %copy-done.2), kind=kOutput, calls=%fused_computation.78 | convolution fusion | flops 1076625408 | bytes 12058624 | tf_op jit(solution)/shard_map/dot_general | solution.py:139
  286.8 1.7 copy-done.5
  288.5 4.4 %fusion = bf16[1,512,2048]{2,1,0:T(8,128)(2,1)} fusion(bf16[512,640]{0,1:T(8,128)(2,1)} %copy-done.6, bf16[1,640,2048]{2,1,0:T(8,128)(2,1)S(1)} %copy-done.5), kind=kOutput, calls=%fused_computation.9 | convolution fusion | flops 1343225856 | bytes 5373952 | tf_op jit(solution)/shard_map/xfr,xrd->xfd/dot_general | solution.py:42
  292.9 3.3 fusion.2
  296.3 1.4 collective-permute-start.1
  297.7 3.2 fusion.1
  301.0 1.2 fusion.35
  302.2 1.0 fusion.37
  303.2 87.2 %reduce-scatter.2.cloned.1.call-done = f32[128,1024]{1,0:T(8,128)} async-done(((f32[2048,1024]{1,0:T(8,128)}), f32[128,1024]{1,0:T(8,128)}) %reduce-scatter.2.cloned.1.call-update) | async-done | bytes 524304 | tf_op jit(solution)/shard_map/reduce_scatter | solution.py:138
  (76 shorter events, 3.1 us)
Async XLA Ops:
  7.2 101.0 %copy-start = (bf16[1,512,2048]{2,1,0:T(8,128)(2,1)S(1)}, bf16[1,512,2048]{2,1,0:T(8,128)(2,1)}, u32[]{:S(2)}) copy-start(bf16[1,512,2048]{2,1,0:T(8,128)(2,1)} %param.16) | copy-start | bytes 6291460
  14.4 4.4 %copy-start.3 = (bf16[256,2048]{1,0:T(8,128)(2,1)S(1)}, bf16[256,2048]{1,0:T(8,128)(2,1)}, u32[]{:S(2)}) copy-start(bf16[256,2048]{1,0:T(8,128)(2,1)} %param.12) | copy-start | bytes 3145732
  22.9 10.3 %copy-start.2 = (bf16[256,2048]{1,0:T(8,128)(2,1)S(1)}, bf16[256,2048]{1,0:T(8,128)(2,1)}, u32[]{:S(2)}) copy-start(bf16[256,2048]{1,0:T(8,128)(2,1)} %param.13) | copy-start | bytes 3145732
  25.7 34.8 %all-to-all-start = ((bf16[16,40,1024]{2,1,0:T(8,128)(2,1)}), bf16[16,40,1024]{2,1,0:T(8,128)(2,1)}, u32[]{:S(2)}, u32[]{:S(2)}) async-start(bf16[16,40,1024]{2,1,0:T(8,128)(2,1)} %dynamic-slice_select_fusion), calls=%async_computation | async-start | bytes 2621440 | tf_op jit(solution)/shard_map/all_to_all | solution.py:89
  33.1 69.9 %all-gather.5.cloned.1.call-start = ((), (), s32[]{:S(2)}) async-start(), calls=%async_computation.5 | async-start | bytes 3932160 | tf_op jit(solution)/shard_map/all_gather | solution.py:93
  60.5 83.1 %all-gather.7.cloned.1.call-start = ((), (), s32[]{:S(2)}) async-start(), calls=%async_computation.6 | async-start | bytes 3932160 | tf_op jit(solution)/shard_map/all_gather | solution.py:94
  101.5 155.7 %all-gather.11.cloned.1.call-start = ((), (), s32[]{:S(2)}) async-start(), calls=%async_computation.9 | async-start | bytes 4456448 | tf_op jit(solution)/shard_map/all_gather | solution.py:133
  103.1 5.1 %copy-start.4 = (bf16[1,640,2048]{2,1,0:T(8,128)(2,1)S(1)}, bf16[1,640,2048]{2,1,0:T(8,128)(2,1)}, u32[]{:S(2)}) copy-start(bf16[1,640,2048]{2,1,0:T(8,128)(2,1)} %all-gather.5.cloned.1.call-done) | copy-start | bytes 7864324
  149.1 1.6 copy-start.6
  149.1 1.6 copy-start.12
  149.1 2.1 copy-start.18
  205.3 32.9 %all-to-all-start.3 = ((bf16[16,2,20480]{2,1,0:T(2,128)(2,1)}), bf16[16,2,20480]{2,1,0:T(2,128)(2,1)S(1)}, u32[]{:S(2)}, u32[]{:S(2)}) async-start(bf16[16,2,20480]{2,1,0:T(2,128)(2,1)} %reshape.230), calls=%async_computation.3 | async-start | bytes 2621440 | tf_op jit(solution)/shard_map/all_to_all | solution.py:109
  210.9 65.0 %all-gather.9.cloned.1.call-start = ((), (), s32[]{:S(2)}) async-start(), calls=%async_computation.7 | async-start | bytes 1572864 | tf_op jit(solution)/shard_map/all_gather | solution.py:114
  246.9 5.2 %copy-start.7 = (bf16[256,1024]{1,0:T(8,128)(2,1)S(1)}, bf16[256,1024]{1,0:T(8,128)(2,1)}, u32[]{:S(2)}) copy-start(bf16[256,1024]{1,0:T(8,128)(2,1)} %param.20) | copy-start | bytes 1572868
  246.9 5.2 %copy-start.9 = (bf16[256,1024]{1,0:T(8,128)(2,1)S(1)}, bf16[256,1024]{1,0:T(8,128)(2,1)}, u32[]{:S(2)}) copy-start(bf16[256,1024]{1,0:T(8,128)(2,1)} %param.21) | copy-start | bytes 1572868
  248.4 6.8 %copy-start.16 = (f32[3,1024]{1,0:T(4,128)S(1)}, f32[3,1024]{1,0:T(4,128)}, u32[]{:S(2)}) copy-start(f32[3,1024]{1,0:T(4,128)} %param.22) | copy-start | bytes 36868
  252.1 138.3 %reduce-scatter.2.cloned.1.call-start = ((), (), s32[]{:S(2)}) async-start(), calls=%async_computation.8 | async-start | bytes 8912896 | tf_op jit(solution)/shard_map/reduce_scatter | solution.py:138
  252.3 3.7 collective-permute-start
  275.9 6.2 %copy-start.11 = (bf16[256,2048]{1,0:T(8,128)(2,1)S(1)}, bf16[256,2048]{1,0:T(8,128)(2,1)}, u32[]{:S(2)}) copy-start(bf16[256,2048]{1,0:T(8,128)(2,1)} %all-gather.9.cloned.1.call-done) | copy-start | bytes 3145732
  275.9 6.2 %copy-start.15 = (bf16[256,1024]{1,0:T(8,128)(2,1)S(1)}, bf16[256,1024]{1,0:T(8,128)(2,1)}, u32[]{:S(2)}) copy-start(bf16[256,1024]{1,0:T(8,128)(2,1)} %param.19) | copy-start | bytes 1572868
  286.8 1.7 copy-start.5
  288.5 4.4 %copy-start.17 = (bf16[1,640,2048]{2,1,0:T(8,128)(2,1)S(1)}, bf16[1,640,2048]{2,1,0:T(8,128)(2,1)}, u32[]{:S(2)}) copy-start(bf16[1,640,2048]{2,1,0:T(8,128)(2,1)} %all-gather.7.cloned.1.call-done) | copy-start | bytes 7864324
  288.5 4.4 %copy-start.19 = (f32[640,512]{1,0:T(8,128)S(1)}, f32[640,512]{1,0:T(8,128)}, u32[]{:S(2)}) copy-start(f32[640,512]{1,0:T(8,128)} %fusion.9) | copy-start | bytes 3932164
  288.5 4.4 %copy-start.20 = (f32[640,512]{1,0:T(8,128)S(1)}, f32[640,512]{1,0:T(8,128)}, u32[]{:S(2)}) copy-start(f32[640,512]{1,0:T(8,128)} %fusion.11) | copy-start | bytes 3932164
  292.9 3.4 copy-start.14
  292.9 4.8 %copy-start.13 = (bf16[512,640]{0,1:T(8,128)(2,1)S(1)}, bf16[512,640]{0,1:T(8,128)(2,1)}, u32[]{:S(2)}) copy-start(bf16[512,640]{0,1:T(8,128)(2,1)} %copy-done.12) | copy-start | bytes 1966084
  296.3 4.7 %copy-start.8 = (bf16[256,1024]{1,0:T(8,128)(2,1)S(1)}, bf16[256,1024]{1,0:T(8,128)(2,1)}, u32[]{:S(2)}) copy-start(bf16[256,1024]{1,0:T(8,128)(2,1)} %param.20) | copy-start | bytes 1572868
  296.3 4.6 %collective-permute-start.1 = (bf16[2,1024]{1,0:T(2,128)(2,1)S(1)}, bf16[2,1024]{1,0:T(2,128)(2,1)S(1)}, u32[]{:S(2)}, u32[]{:S(2)}) collective-permute-start(bf16[2,1024]{1,0:T(2,128)(2,1)S(1)} %slice.68), channel_id=1, source_target_pairs={{2,0},{4,2},{6,4},{8,6},{10,8},{12,10},{14,12},{16,14},{18,16},{20... | collective-permute-start | bytes 12296 | tf_op jit(solution)/shard_map/ppermute | solution.py:13
  301.0 1.2 copy-start.10
  301.0 89.4 %copy-start.1 = (bf16[1,512,2048]{2,1,0:T(8,128)(2,1)S(1)}, bf16[1,512,2048]{2,1,0:T(8,128)(2,1)}, u32[]{:S(2)}) copy-start(bf16[1,512,2048]{2,1,0:T(8,128)(2,1)} %param.16) | copy-start | bytes 6291460
Sparse Core Ops, SparseCore 0:
  60.6 42.3 all-gather.4
  104.6 38.9 all-gather.6
  145.8 52.3 all-gather.10
  252.2 23.7 all-gather.8
  286.9 103.4 reduce-scatter.1
where the time goes:
time: 402 us; the launch traced here: 397 us
  waiting for transfers between devices  191 us (48%)
  blocking collectives  73.6 us (18%)
  matrix products  38 us (9%)
  local copies, waits for them, and re-layouts  36.2 us (9%)
  other arithmetic  26 us (6%)
  starting transfers between devices  17.9 us (4%)
  between operations  14.6 us (4%)
    reduce_scatter x1, waiting for transfers between devices, local(): lax.psum_scatter(lax.dot_general(columns, mixed, (((0,), (0,)), ((), ()))...  87.2 us
    all_to_all x1, blocking collectives, local(): lax.all_to_all(part_grads, 'sp', split_axis=0, concat_axis=1, tiled=True)  39.3 us
    all_to_all x1, blocking collectives, local(): lax.all_to_all(input_part.reshape(local_experts * slot_count, tp_count, w...  34.3 us
    all_gather x1, waiting for transfers between devices, local(): lax.all_gather(cotan_part, 'tp', axis=2, tiled=True)  32.8 us
    all_to_all x1, waiting for transfers between devices, local(): lax.all_to_all(slot_sums, 'sp', split_axis=1, concat_axis=0, tiled=True)  27 us
    all_to_all x1, waiting for transfers between devices, local(): lax.all_to_all(part_rows, 'sp', split_axis=0, concat_axis=1, tiled=True)  23.1 us
    all_gather x1, waiting for transfers between devices, local(): full_rows = lax.all_gather(row_grads, 'tp', axis=1, tiled=True)  18.8 us
    unnamed x48, local copies, waits for them, and re-layouts  12 us
  transfers between devices with their start and end apart: 9, of which 7 were waited for; matrix products, arithmetic and copies ran while one was open for 17% of the time, Pallas kernels for 0%

commit v1 on v0

v1 whole, which is shorter than its diff:
```python
import functools

import jax
import jax.numpy as jnp
from jax import lax
from jax.experimental import pallas as pl
from jax.experimental.pallas import tpu as pltpu
from jax.sharding import PartitionSpec as P

LIMIT = 7.0
ALPHA = 1.702
BF16 = jnp.bfloat16
F32 = jnp.float32
MESH = pl.DeviceIdType.MESH
VMEM_LIMIT = 56 * 1024 * 1024
VMEM_SPEC = pl.BlockSpec(memory_space=pltpu.VMEM)


def from_behind(value, axis, by):
    count = lax.axis_size(axis)
    pairs = [(i, i + by) for i in range(count) if 0 <= i + by < count]
    return lax.ppermute(value, axis, pairs)


def remote(src, dst, send, recv, sp, tp):
    return pltpu.make_async_remote_copy(
        src_ref=src,
        dst_ref=dst,
        send_sem=send,
        recv_sem=recv,
        device_id=(sp, tp),
        device_id_type=MESH,
    )


def greet(peers):
    barrier = pltpu.get_barrier_semaphore()
    for peer in peers:
        pl.semaphore_signal(barrier, inc=1, device_id=peer, device_id_type=MESH)
    pl.semaphore_wait(barrier, len(peers))


def dispatch_kernel(
    n, p, rows_ref, grads_ref, routed, cotan, local_sem, send, recv, relay_send, relay_recv
):
    me, t = lax.axis_index("sp"), lax.axis_index("tp")
    width = rows_ref.shape[2]
    others = [lax.rem(me + k, n) for k in range(1, n)]
    sides = [lax.rem(t + k, p) for k in range(1, p)]
    greet([(o, t) for o in others] + [(me, s) for s in sides])
    mine = pl.ds(pl.multiple_of(t * width, width), width)
    pairs = ((rows_ref, routed), (grads_ref, cotan))
    started = []
    for a, (src, dst) in enumerate(pairs):
        own = pltpu.make_async_copy(src.at[me], dst.at[me, :, mine], local_sem.at[a])
        own.start()
        started.append(own)
    sends = []
    for a, (src, dst) in enumerate(pairs):
        for k in range(1, n):
            to = others[k - 1]
            copy = remote(
                src.at[to], dst.at[me, :, mine], send.at[a, k], recv.at[a, k], to, t
            )
            copy.start()
            sends.append(copy)
        for j in range(1, p):
            copy = remote(
                src.at[me],
                dst.at[me, :, mine],
                relay_send.at[a, 0, j],
                relay_recv.at[a, 0, j],
                me,
                sides[j - 1],
            )
            copy.start()
            sends.append(copy)
    for a, (src, dst) in enumerate(pairs):
        for k in range(1, n):
            frm = lax.rem(me - k + n, n)
            landed = dst.at[frm, :, mine]
            remote(src.at[frm], landed, send.at[a, k], recv.at[a, k], frm, t).wait_recv()
            for j in range(1, p):
                copy = remote(
                    landed, landed, relay_send.at[a, k, j], relay_recv.at[a, k, j], me, sides[j - 1]
                )
                copy.start()
                sends.append(copy)
    for own in started:
        own.wait()
    for a, (src, dst) in enumerate(pairs):
        for k in range(n):
            frm = lax.rem(me - k + n, n)
            for j in range(1, p):
                side = lax.rem(t - j + p, p)
                theirs = pl.ds(pl.multiple_of(side * width, width), width)
                landed = dst.at[frm, :, theirs]
                remote(
                    landed, landed, relay_send.at[a, k, j], relay_recv.at[a, k, j], me, side
                ).wait_recv()
    for copy in sends:
        copy.wait_send()


def dispatch(rows, grads, n, p):
    count, cap, width = rows.shape
    out = jax.ShapeDtypeStruct((n, cap, width * p), BF16)
    return pl.pallas_call(
        functools.partial(dispatch_kernel, n, p),
        out_shape=(out, out),
        in_specs=[VMEM_SPEC] * 2,
        out_specs=(VMEM_SPEC, VMEM_SPEC),
        scratch_shapes=[
            pltpu.SemaphoreType.DMA((2,)),
            pltpu.SemaphoreType.DMA((2, n)),
            pltpu.SemaphoreType.DMA((2, n)),
            pltpu.SemaphoreType.DMA((2, n, p)),
            pltpu.SemaphoreType.DMA((2, n, p)),
        ],
        compiler_params=pltpu.CompilerParams(
            collective_id=0, has_side_effects=True, vmem_limit_bytes=VMEM_LIMIT
        ),
    )(rows, grads)


def return_kernel(
    n,
    p,
    part,
    pick,
    full,
    beside,
    stage,
    back,
    total,
    side_send,
    side_recv,
    send,
    recv,
    row_send,
    row_recv,
):
    me, t = lax.axis_index("sp"), lax.axis_index("tp")
    width = stage.shape[2]
    others = [lax.rem(me + k, n) for k in range(1, n)]
    sides = [lax.rem(t + k, p) for k in range(1, p)]
    greet([(o, t) for o in others] + [(me, s) for s in sides])
    sends = []
    for k in list(range(1, n)) + [0]:
        to = lax.rem(me + k, n)
        for j in range(1, p):
            side = sides[j - 1]
            theirs = pl.ds(pl.multiple_of(side * width, width), width)
            copy = remote(
                part.at[to, :, theirs],
                beside.at[k, j],
                side_send.at[k, j],
                side_recv.at[k, j],
                me,
                side,
            )
            copy.start()
            sends.append(copy)
    mine = pl.ds(pl.multiple_of(t * width, width), width)
    for k in list(range(1, n)) + [0]:
        to = lax.rem(me + k, n)
        value = part[to, :, mine].astype(F32)
        for j in range(1, p):
            side = lax.rem(t - j + p, p)
            remote(
                part.at[to, :, mine], beside.at[k, j], side_send.at[k, j], side_recv.at[k, j], me, side
            ).wait_recv()
            value = value + beside[k, j].astype(F32)
        stage[k] = value.astype(BF16)
        if k > 0:
            copy = remote(stage.at[k], back.at[k], send.at[k], recv.at[k], to, t)
            copy.start()
            sends.append(copy)
    total[...] = jnp.dot(pick[me], stage[0], preferred_element_type=F32)
    for k in range(1, n):
        frm = lax.rem(me - k + n, n)
        remote(stage.at[k], back.at[k], send.at[k], recv.at[k], frm, t).wait_recv()
        total[...] += jnp.dot(pick[frm], back[k], preferred_element_type=F32)
    full[:, mine] = total[...].astype(BF16)
    for j in range(1, p):
        copy = remote(
            full.at[:, mine], full.at[:, mine], row_send.at[j], row_recv.at[j], me, sides[j - 1]
        )
        copy.start()
        sends.append(copy)
    for j in range(1, p):
        side = lax.rem(t - j + p, p)
        theirs = pl.ds(pl.multiple_of(side * width, width), width)
        remote(
            full.at[:, theirs], full.at[:, theirs], row_send.at[j], row_recv.at[j], me, side
        ).wait_recv()
    for copy in sends:
        copy.wait_send()


def return_rows(part, pick, n, p):
    count, cap, whole = part.shape
    tokens = pick.shape[1]
    width = whole // p
    return pl.pallas_call(
        functools.partial(return_kernel, n, p),
        out_shape=jax.ShapeDtypeStruct((tokens, whole), BF16),
        in_specs=[VMEM_SPEC] * 2,
        out_specs=VMEM_SPEC,
        scratch_shapes=[
            pltpu.VMEM((n, p, cap, width), BF16),
            pltpu.VMEM((n, cap, width), BF16),
            pltpu.VMEM((n, cap, width), BF16),
            pltpu.VMEM((tokens, width), F32),
            pltpu.SemaphoreType.DMA((n, p)),
            pltpu.SemaphoreType.DMA((n, p)),
            pltpu.SemaphoreType.DMA((n,)),
            pltpu.SemaphoreType.DMA((n,)),
            pltpu.SemaphoreType.DMA((p,)),
            pltpu.SemaphoreType.DMA((p,)),
        ],
        compiler_params=pltpu.CompilerParams(
            collective_id=1, has_side_effects=True, vmem_limit_bytes=VMEM_LIMIT
        ),
    )(part, pick)


def scatter_kernel(
    m,
    chunks,
    terms,
    out,
    core_in,
    core_sum,
    pair_in,
    pair_sum,
    far_in,
    core_send,
    core_recv,
    pair_send,
    pair_recv,
    far_send,
    far_recv,
):
    me, t = lax.axis_index("sp"), lax.axis_index("tp")
    c = lax.rem(me, 2)
    x = lax.rem(me // 2, 2)
    z = me // 4
    core_peer = me + 1 - 2 * c
    pair_peer = me + 2 - 4 * x
    far = [lax.rem(z + k, m) * 4 + x * 2 + c for k in range(1, m)]
    back = [lax.rem(z - k + m, m) * 4 + x * 2 + c for k in range(1, m)]
    greet([(core_peer, t), (pair_peer, t)] + [(f, t) for f in far])
    rows = terms.shape[3] // chunks
    cuts = [pl.ds(i * rows, rows) for i in range(chunks)]
    sends = []
    order = [lax.rem(z + k, m) for k in list(range(1, m)) + [0]]
    for i, cut in enumerate(cuts):
        for q in range(2):
            xx = 1 - x if q == 0 else x
            for k in range(m):
                copy = remote(
                    terms.at[order[k], xx, 1 - c, cut],
                    core_in.at[i, q, k],
                    core_send.at[i, q, k],
                    core_recv.at[i, q, k],
                    core_peer,
                    t,
                )
                copy.start()
                sends.append(copy)
    for i, cut in enumerate(cuts):
        for q in range(2):
            xx = 1 - x if q == 0 else x
            for k in range(m):
                remote(
                    terms.at[order[k], xx, 1 - c, cut],
                    core_in.at[i, q, k],
                    core_send.at[i, q, k],
                    core_recv.at[i, q, k],
                    core_peer,
                    t,
                ).wait_recv()
                core_sum[i, q, k] = (
                    terms[order[k], xx, c, cut].astype(F32) + core_in[i, q, k].astype(F32)
                ).astype(BF16)
                if q == 0:
                    copy = remote(
                        core_sum.at[i, 0, k],
                        pair_in.at[i, k],
                        pair_send.at[i, k],
                        pair_recv.at[i, k],
                        pair_peer,
                        t,
                    )
                    copy.start()
                    sends.append(copy)
    for i, cut in enumerate(cuts):
        for k in range(m):
            remote(
                core_sum.at[i, 0, k],
                pair_in.at[i, k],
                pair_send.at[i, k],
                pair_recv.at[i, k],
                pair_peer,
                t,
            ).wait_recv()
            value = core_sum[i, 1, k].astype(F32) + pair_in[i, k].astype(F32)
            if k < m - 1:
                pair_sum[i, k] = value.astype(BF16)
                copy = remote(
                    pair_sum.at[i, k],
                    far_in.at[i, k],
                    far_send.at[i, k],
                    far_recv.at[i, k],
                    far[k],
                    t,
                )
                copy.start()
                sends.append(copy)
            else:
                out[cut] = value
    for i, cut in enumerate(cuts):
        for k in range(m - 1):
            remote(
                pair_sum.at[i, k],
                far_in.at[i, k],
                far_send.at[i, k],
                far_recv.at[i, k],
                back[k],
                t,
            ).wait_recv()
            out[cut] += far_in[i, k].astype(F32)
    for copy in sends:
        copy.wait_send()


def scatter_sum(terms, n):
    total, width = terms.shape
    rows = total // n
    m = n // 4
    chunks = 4
    part = rows // chunks
    return pl.pallas_call(
        functools.partial(scatter_kernel, m, chunks),
        out_shape=jax.ShapeDtypeStruct((rows, width), F32),
        in_specs=[VMEM_SPEC],
        out_specs=VMEM_SPEC,
        scratch_shapes=[
            pltpu.VMEM((chunks, 2, m, part, width), BF16),
            pltpu.VMEM((chunks, 2, m, part, width), BF16),
            pltpu.VMEM((chunks, m, part, width), BF16),
            pltpu.VMEM((chunks, m, part, width), BF16),
            pltpu.VMEM((chunks, m, part, width), BF16),
            pltpu.SemaphoreType.DMA((chunks, 2, m)),
            pltpu.SemaphoreType.DMA((chunks, 2, m)),
            pltpu.SemaphoreType.DMA((chunks, m)),
            pltpu.SemaphoreType.DMA((chunks, m)),
            pltpu.SemaphoreType.DMA((chunks, m)),
            pltpu.SemaphoreType.DMA((chunks, m)),
        ],
        compiler_params=pltpu.CompilerParams(
            collective_id=2, has_side_effects=True, vmem_limit_bytes=VMEM_LIMIT
        ),
    )(terms.reshape(m, 2, 2, rows, width))


def slot_positions(route_ids, experts, capacity):
    tokens, top_count = route_ids.shape
    flat = route_ids.reshape(-1)
    onehot = flat[:, None] == jnp.arange(experts, dtype=jnp.int32)[None, :]
    index = jnp.arange(flat.shape[0], dtype=jnp.int32)
    earlier = (index[:, None] > index[None, :]).astype(BF16)
    before = jnp.dot(earlier, onehot.astype(BF16), preferred_element_type=F32)
    slot_rank = jnp.sum(jnp.where(onehot, before, 0.0), axis=1).astype(jnp.int32)
    return (flat * capacity + slot_rank).reshape(tokens, top_count)


def local(
    moe_input,
    out_grad,
    route_ids,
    route_weights,
    gate_weight,
    lin_weight,
    down_weight,
    outer_gate,
    inner_gate,
    conv_input,
    conv_taps,
    out_proj,
):
    n = lax.axis_size("sp")
    p = lax.axis_size("tp")
    local_experts = gate_weight.shape[0]
    assert local_experts == 1
    experts = local_experts * n
    tokens, top_count = route_ids.shape
    width = moe_input.shape[1]
    width_dev = width // p
    capacity = 5 * tokens // (2 * experts)
    capacity = -(-capacity // 8) * 8
    slots = experts * capacity
    position = slot_positions(route_ids, experts, capacity)
    slot_index = jnp.arange(slots, dtype=jnp.int32)
    hits = [position[:, k][None, :] == slot_index[:, None] for k in range(top_count)]
    taken = functools.reduce(jnp.logical_or, hits)
    slot_weight = sum(
        jnp.sum(jnp.where(hits[k], route_weights[:, k][None, :], 0.0), axis=1)
        for k in range(top_count)
    )
    select = taken.astype(BF16)
    column_start = lax.axis_index("tp") * width_dev
    part_rows = lax.dynamic_slice_in_dim(moe_input, column_start, width_dev, 1)
    part_grads = lax.dynamic_slice_in_dim(out_grad, column_start, width_dev, 1)
    send_rows = jnp.dot(select, part_rows, preferred_element_type=F32).astype(BF16)
    send_grads = (
        slot_weight[:, None] * jnp.dot(select, part_grads, preferred_element_type=F32)
    ).astype(BF16)
    routed, cotan = dispatch(
        send_rows.reshape(experts, capacity, width_dev),
        send_grads.reshape(experts, capacity, width_dev),
        n,
        p,
    )
    routed = routed.reshape(slots, width)
    cotan = cotan.reshape(slots, width)
    gate_w, lin_w, down_w = gate_weight[0], lin_weight[0], down_weight[0]

    def product(a, b, left, right):
        return lax.dot_general(a, b, (((left,), (right,)), ((), ())), preferred_element_type=F32)

    gate_pre = product(gate_w, routed, 1, 1)
    lin_pre = product(lin_w, routed, 1, 1)
    act_grad = product(down_w, cotan, 1, 1)
    gate_cut = jnp.minimum(gate_pre, LIMIT)
    lin_cut = jnp.clip(lin_pre, -LIMIT, LIMIT)
    sigma = jax.nn.sigmoid(ALPHA * gate_cut)
    act = (gate_cut * sigma * (lin_cut + 1.0)).astype(BF16)
    slope = sigma * (1.0 + ALPHA * gate_cut * (1.0 - sigma))
    gate_cot = jnp.where(gate_pre < LIMIT, act_grad * (lin_cut + 1.0) * slope, 0.0).astype(BF16)
    lin_cot = jnp.where(jnp.abs(lin_pre) < LIMIT, act_grad * gate_cut * sigma, 0.0).astype(BF16)
    input_part = (product(gate_cot, gate_w, 0, 0) + product(lin_cot, lin_w, 0, 0)).astype(BF16)
    down_grad = product(act, cotan, 1, 0).astype(BF16)[None]
    gate_grad = product(gate_cot, routed, 1, 0).astype(BF16)[None]
    lin_grad = product(lin_cot, routed, 1, 0).astype(BF16)[None]

    expert_slot = slot_index.reshape(experts, 1, capacity)
    pick = functools.reduce(
        jnp.logical_or,
        [position[:, k][None, :, None] == expert_slot for k in range(top_count)],
    ).astype(BF16)
    full_rows = return_rows(input_part.reshape(n, capacity, width), pick, n, p)
    stream_grad = (out_grad.astype(F32) + full_rows.astype(F32)).astype(BF16)

    tap_count = conv_taps.shape[0]
    conv_values = (inner_gate.astype(F32) * conv_input.astype(F32)).astype(BF16)
    prior_rows = from_behind(conv_values[tokens - (tap_count - 1) :], "sp", 1)
    extended = jnp.concatenate([prior_rows, conv_values], axis=0).astype(F32)
    convolved = jnp.zeros((tokens, width_dev), F32)
    for tap_index in range(tap_count):
        convolved = (
            convolved + conv_taps[tap_index][None, :] * extended[tap_index : tap_index + tokens]
        )
    mixed = (outer_gate.astype(F32) * convolved).astype(BF16)
    proj = lax.all_gather(out_proj, "sp", axis=1, tiled=True)
    mixed_grad = product(stream_grad, proj, 1, 1)
    out_proj_grad = scatter_sum(product(stream_grad, mixed, 0, 0).astype(BF16), n)
    outer_gate_grad = (mixed_grad * convolved).astype(BF16)
    conv_cot = (mixed_grad * outer_gate.astype(F32)).astype(BF16)
    later_rows = from_behind(conv_cot[: tap_count - 1], "sp", -1)
    extended_cot = jnp.concatenate([conv_cot, later_rows], axis=0).astype(F32)
    value_grad = jnp.zeros((tokens, width_dev), F32)
    for tap_index in range(tap_count):
        first_row = tap_count - 1 - tap_index
        value_grad = (
            value_grad
            + conv_taps[tap_index][None, :] * extended_cot[first_row : first_row + tokens]
        )
    inner_gate_grad = (value_grad * conv_input.astype(F32)).astype(BF16)
    conv_input_grad = (value_grad * inner_gate.astype(F32)).astype(BF16)
    return (
        gate_grad,
        lin_grad,
        down_grad,
        out_proj_grad,
        outer_gate_grad,
        inner_gate_grad,
        conv_input_grad,
    )


def solution(mesh):
    placed = (
        P("sp", None),
        P("sp", None),
        P("sp", None),
        P("sp", None),
        P("sp", "tp", None),
        P("sp", "tp", None),
        P("sp", "tp", None),
        P("sp", "tp"),
        P("sp", "tp"),
        P("sp", "tp"),
        P(None, "tp"),
        P("tp", "sp"),
    )
    return jax.shard_map(
        local,
        mesh=mesh,
        in_specs=placed,
        out_specs=(
            P("sp", "tp", None),
            P("sp", "tp", None),
            P("sp", "tp", None),
            P("sp", "tp"),
            P("sp", "tp"),
            P("sp", "tp"),
            P("sp", "tp"),
        ),
        check_vma=False,
    )
```

time: 402 us -> 268 us (0.67); the launches traced: 397 us -> 268 us
  Pallas kernels: 0 us -> 203 us
  waiting for transfers between devices: 191 us -> 0.69 us
  blocking collectives: 73.6 us -> 0 us
  local copies, waits for them, and re-layouts: 36.2 us -> 3.75 us
  other arithmetic: 26 us -> 6.5 us
  starting transfers between devices: 17.9 us -> 3.73 us
    pallas_call x0 -> x3, Pallas kernels: none -> 203 us  [the longest x1 97.4 us: dispatch(): pl.pallas_call(functools.partial(dispatch_kernel, n, p), out_shape=(out,...]
    reduce_scatter x1 -> x0, waiting for transfers between devices: 87.2 us -> none  [local(): lax.psum_scatter(lax.dot_general(columns, mixed, (((0,), (0,)), ((), ()))...]
    all_to_all x2 -> x0, blocking collectives: 73.6 us -> none  [the longest x1 39.3 us: local(): lax.all_to_all(part_grads, 'sp', split_axis=0, concat_axis=1, tiled=True)]
    all_gather x4 -> x1, waiting for transfers between devices: 52.4 us -> 0.01 us  [local(): proj = lax.all_gather(out_proj, 'sp', axis=1, tiled=True)]
    all_to_all x2 -> x0, waiting for transfers between devices: 50.1 us -> none  [the longest x1 27 us: local(): lax.all_to_all(slot_sums, 'sp', split_axis=1, concat_axis=0, tiled=True)]
    gather x5 -> x0, local copies, waits for them, and re-layouts: 16.8 us -> none  [the longest x2 4.33 us: local(): returned.reshape(experts * capacity, width_dev)[position]]
    all_to_all x2 -> x0, starting transfers between devices: 13 us -> none  [the longest x1 7.43 us: local(): lax.all_to_all(part_rows, 'sp', split_axis=0, concat_axis=1, tiled=True)]
    unnamed x1 -> x0, other arithmetic: 9.64 us -> none
  transfers between devices with their start and end apart: 9 -> 3, of which waited for: 7 -> 0; matrix products, arithmetic and copies ran while one was open for 17% -> 13% of each run, Pallas kernels for 0% -> 76%
where the time goes in v1:
time: 268 us
  Pallas kernels  203 us (76%)
  matrix products  35.6 us (13%)
  between operations  14.3 us (5%)
  other arithmetic  6.5 us (2%)
  local copies, waits for them, and re-layouts  3.75 us (1%)
  starting transfers between devices  3.73 us (1%)
    pallas_call x1, Pallas kernels, dispatch(): pl.pallas_call(functools.partial(dispatch_kernel, n, p), out_shape=(out,...  97.4 us
    pallas_call x1, Pallas kernels, return_rows(): pl.pallas_call(functools.partial(return_kernel, n, p), out_shape=jax.Shap...  64.5 us
    pallas_call x1, Pallas kernels, scatter_sum(): pl.pallas_call(functools.partial(scatter_kernel, m, chunks), out_shape=ja...  41.2 us
    dot_general x10, matrix products, product(): lax.dot_general(a, b, (((left,), (right,)), ((), ())), preferred_element_...  31.1 us
  transfers between devices with their start and end apart: 3, of which 0 were waited for; matrix products, arithmetic and copies ran while one was open for 13% of the time, Pallas kernels for 76%

profile of v1, /device:TPU:0, one launch (start us, length us, event | category | flops | bytes accessed | tf_op | source)
XLA Modules:
  0.0 267.7 jit_solution(18263774458922404655)
XLA Ops:
  7.2 0.0 copy-start
  7.2 0.0 copy-start.11
  7.2 0.0 copy-start.12
  7.2 0.0 all-gather.2.cloned.1.call-start
  7.2 0.7 all-gather.2.cloned.1.call-update
  7.9 1.5 fusion.28
  9.4 0.0 copy-start.4
  9.4 0.8 copy-done.4
  10.2 2.4 collective-permute-start
  12.7 0.8 copy.28
  13.5 0.1 eq.71
  13.6 0.3 fusion.24
  13.9 0.1 convert_element_type.89
  14.0 0.1 copy.29
  14.1 0.0 copy-done.11
  14.2 0.2 select_reduce_fusion
  14.4 2.6 convolution_convert_fusion.4
  17.1 0.0 copy-done.3
  17.1 1.6 multiply_convert_fusion
  18.6 97.4 %shard_map.171 = (bf16[16,40,2048]{2,1,0:T(8,128)(2,1)}, bf16[16,40,2048]{2,1,0:T(8,128)(2,1)}) custom-call(bf16[16,40,1024]{2,1,0:T(8,128)(2,1)} %bitcast.95, bf16[16,40,1024]{2,1,0:T(8,128)(2,1)} %bitcast.97), custom_call_target="tpu_custom_call" | custom-call | tf_op jit(solution)/shard_map/pallas_call | solution.py:108
  116.1 1.4 or_convert_fusion.pick
  117.4 0.0 copy-done
  117.4 3.4 %fusion.10 = f32[640,512]{1,0:T(8,128)S(1)} fusion(bf16[640,2048]{1,0:T(8,128)(2,1)} %bitcast.91, bf16[1,512,2048]{2,1,0:T(8,128)(2,1)S(1)} %copy-done), kind=kOutput, calls=%fused_computation.16 | convolution fusion | flops 1342177280 | bytes 6029312 | tf_op jit(solution)/shard_map/dot_general | solution.py:431
  120.9 0.0 copy-start.14
  120.9 1.6 fusion.4
  122.5 0.2 copy-done.13
  122.6 0.6 copy-done.14
  123.3 2.3 fusion.17
  125.6 3.2 %fusion.1 = bf16[1,512,2048]{2,1,0:T(8,128)(2,1)} fusion(bf16[512,640]{0,1:T(8,128)(2,1)S(1)} %get-tuple-element.15, bf16[640,2048]{1,0:T(8,128)(2,1)S(1)} %bitcast.93), kind=kOutput, calls=%fused_computation.6 | convolution fusion | flops 1343225856 | bytes 5373952 | tf_op jit(solution)/shard_map/dot_general | solution.py:431
  128.8 3.2 %fusion = bf16[1,512,2048]{2,1,0:T(8,128)(2,1)} fusion(bf16[512,640]{0,1:T(8,128)(2,1)S(1)} %get-tuple-element.16, bf16[640,2048]{1,0:T(8,128)(2,1)S(1)} %bitcast.94), kind=kOutput, calls=%fused_computation.5 | convolution fusion | flops 1343225856 | bytes 5373952 | tf_op jit(solution)/shard_map/dot_general | solution.py:431
  132.0 1.6 fusion.8
  133.5 3.0 %add_convert_fusion = bf16[640,2048]{1,0:T(8,128)(2,1)} fusion(f32[640,2048]{1,0:T(8,128)S(1)} %fusion.8, bf16[512,640]{0,1:T(8,128)(2,1)S(1)} %get-tuple-element.15, bf16[1,512,2048]{2,1,0:T(8,128)(2,1)S(1)} %copy-done.15), kind=kOutput, calls=%fused_computation | convolution fusion | flops 1344798720 | bytes 10616832 | tf_op jit(solution)/shard_map/dot_general | solution.py:431
  136.6 3.6 %fusion.2 = bf16[1,512,2048]{2,1,0:T(8,128)(2,1)} fusion(bf16[640,2048]{1,0:T(8,128)(2,1)S(1)} %bitcast.115, f32[640,512]{1,0:T(8,128)S(1)} %fusion.10, f32[640,512]{1,0:T(8,128)S(1)} %fusion.4), kind=kOutput, calls=%fused_computation.7 | convolution fusion | flops 1346502656 | bytes 7340032 | tf_op jit(solution)/shard_map/dot_general | solution.py:431
  140.2 0.0 copy-start.5
  140.2 64.5 %shard_map.172 = bf16[256,2048]{1,0:T(8,128)(2,1)} custom-call(bf16[16,40,2048]{2,1,0:T(8,128)(2,1)} %bitcast.96, bf16[16,256,40]{2,1,0:T(8,128)(2,1)} %or_convert_fusion.pick), custom_call_target="tpu_custom_call" | custom-call | tf_op jit(solution)/shard_map/pallas_call | solution.py:205
  204.6 0.0 collective-permute-done
  204.7 1.2 maximum_convert_fusion
  205.8 6.0 %multiply_convert_fusion.1 = (bf16[256,1024]{1,0:T(8,128)(2,1)}, f32[256,1024]{1,0:T(8,128)S(1)}, bf16[256,1024]{1,0:T(8,128)(2,1)S(1)}) fusion(f32[258,1024]{1,0:T(8,128)} %maximum_convert_fusion, f32[1024]{0:T(1024)S(1)} %bitcast.108, f32[1024]{0:T(1024)S(1)} %bitcast.110, f32[1024]{0:T(1024)S(1)} %bitcast.106, bf16[256,1024]{1,0:T(8,128)(2,1)} %param.19, ...), kind=kOutput, calls=%fused_computation.60 | convolution fusion | flops 1078460416 | bytes 12070912 | tf_op jit(solution)/shard_map/dot_general | solution.py:431
  211.8 1.3 collective-permute-start.1
  213.2 3.3 %convolution_convert_fusion = bf16[2048,1024]{1,0:T(8,128)(2,1)} fusion(f32[256,1024]{1,0:T(8,128)S(1)} %get-tuple-element.14, bf16[256,1024]{1,0:T(8,128)(2,1)S(1)} %copy-done.9, bf16[256,2048]{1,0:T(8,128)(2,1)S(1)} %copy-done.2, bf16[256,2048]{1,0:T(8,128)(2,1)S(1)} %copy-done.3), kind=kOutput, calls=%fused_computation.1 | convolution fusion | flops 1078722560 | bytes 7864320 | tf_op jit(solution)/shard_map/dot_general | solution.py:431
  216.5 41.2 %shard_map.173 = f32[128,1024]{1,0:T(8,128)} custom-call(bf16[4,2,2,128,1024]{4,3,2,1,0:T(8,128)(2,1)} %bitcast.90), custom_call_target="tpu_custom_call" | custom-call | tf_op jit(solution)/shard_map/pallas_call | solution.py:344
  257.7 0.0 collective-permute-done.1
  257.7 0.1 maximum_convert_fusion.1
  257.8 0.0 copy-start.8
  257.8 1.2 fusion.27
  259.0 0.9 fusion.29
  260.0 0.1 copy-done.7
  260.1 0.8 copy.32
  (28 shorter events, 0.1 us)
Async XLA Ops:
  7.2 110.3 %copy-start = (bf16[1,512,2048]{2,1,0:T(8,128)(2,1)S(1)}, bf16[1,512,2048]{2,1,0:T(8,128)(2,1)}, u32[]{:S(2)}) copy-start(bf16[1,512,2048]{2,1,0:T(8,128)(2,1)} %param.16) | copy-start | bytes 6291460
  7.2 6.9 %copy-start.11 = (s32[256,2]{0,1:T(2,128)S(1)}, s32[256,2]{0,1:T(2,128)}, u32[]{:S(2)}) copy-start(s32[256,2]{0,1:T(2,128)} %param.14) | copy-start | bytes 6148
  7.2 7.0 %copy-start.12 = (f32[256,2]{0,1:T(2,128)S(1)}, f32[256,2]{0,1:T(2,128)}, u32[]{:S(2)}) copy-start(f32[256,2]{0,1:T(2,128)} %param.15) | copy-start | bytes 6148
  7.2 198.6 %all-gather.2.cloned.1.call-start = ((), (), s32[]{:S(2)}) async-start(), calls=%async_computation | async-start | bytes 4456448 | tf_op jit(solution)/shard_map/all_gather | solution.py:466
  7.9 9.1 %copy-start.3 = (bf16[256,2048]{1,0:T(8,128)(2,1)S(1)}, bf16[256,2048]{1,0:T(8,128)(2,1)}, u32[]{:S(2)}) copy-start(bf16[256,2048]{1,0:T(8,128)(2,1)} %param.13) | copy-start | bytes 3145732
  9.4 0.8 copy-start.4
  10.2 194.4 %collective-permute-start = (bf16[2,1024]{1,0:T(2,128)(2,1)S(1)}, bf16[2,1024]{1,0:T(2,128)(2,1)S(1)}, u32[]{:S(2)}, u32[]{:S(2)}) collective-permute-start(bf16[2,1024]{1,0:T(2,128)(2,1)S(1)} %slice.67), channel_id=1, source_target_pairs={{0,2},{2,4},{4,6},{6,8},{8,10},{10,12},{12,14},{14,16},{16,18},{18... | collective-permute-start | bytes 12296 | tf_op jit(solution)/shard_map/ppermute | solution.py:22
  117.4 3.5 %copy-start.1 = (bf16[16,40,2048]{2,1,0:T(8,128)(2,1)S(1)}, bf16[16,40,2048]{2,1,0:T(8,128)(2,1)}, u32[]{:S(2)}) copy-start(bf16[16,40,2048]{2,1,0:T(8,128)(2,1)} %get-tuple-element.9) | copy-start | bytes 7864324
  117.4 3.5 %copy-start.15 = (bf16[1,512,2048]{2,1,0:T(8,128)(2,1)S(1)}, bf16[1,512,2048]{2,1,0:T(8,128)(2,1)}, u32[]{:S(2)}) copy-start(bf16[1,512,2048]{2,1,0:T(8,128)(2,1)} %param.17) | copy-start | bytes 6291460
  120.9 1.7 copy-start.13
  120.9 2.4 copy-start.14
  136.6 3.6 %copy-start.10 = (f32[3,1024]{1,0:T(4,128)S(1)}, f32[3,1024]{1,0:T(4,128)}, u32[]{:S(2)}) copy-start(f32[3,1024]{1,0:T(4,128)} %param.22) | copy-start | bytes 36868
  140.2 64.5 %copy-start.5 = (bf16[256,1024]{1,0:T(8,128)(2,1)S(1)}, bf16[256,1024]{1,0:T(8,128)(2,1)}, u32[]{:S(2)}) copy-start(bf16[256,1024]{1,0:T(8,128)(2,1)} %copy-done.4) | copy-start | bytes 1572868
  205.8 7.3 %copy-start.2 = (bf16[256,2048]{1,0:T(8,128)(2,1)S(1)}, bf16[256,2048]{1,0:T(8,128)(2,1)}, u32[]{:S(2)}) copy-start(bf16[256,2048]{1,0:T(8,128)(2,1)} %shard_map.172) | copy-start | bytes 3145732
  205.8 7.3 %copy-start.9 = (bf16[256,1024]{1,0:T(8,128)(2,1)S(1)}, bf16[256,1024]{1,0:T(8,128)(2,1)}, u32[]{:S(2)}) copy-start(bf16[256,1024]{1,0:T(8,128)(2,1)} %param.19) | copy-start | bytes 1572868
  211.8 45.9 %collective-permute-start.1 = (bf16[2,1024]{1,0:T(2,128)(2,1)S(1)}, bf16[2,1024]{1,0:T(2,128)(2,1)S(1)}, u32[]{:S(2)}, u32[]{:S(2)}) collective-permute-start(bf16[2,1024]{1,0:T(2,128)(2,1)S(1)} %slice.71), channel_id=1, source_target_pairs={{2,0},{4,2},{6,4},{8,6},{10,8},{12,10},{14,12},{16,14},{18,16},{20... | collective-permute-start | bytes 12296 | tf_op jit(solution)/shard_map/ppermute | solution.py:22
  216.5 41.3 %copy-start.6 = (bf16[256,1024]{1,0:T(8,128)(2,1)S(1)}, bf16[256,1024]{1,0:T(8,128)(2,1)}, u32[]{:S(2)}) copy-start(bf16[256,1024]{1,0:T(8,128)(2,1)} %param.20) | copy-start | bytes 1572868
  257.8 1.2 copy-start.8
  259.0 1.0 copy-start.7
Sparse Core Ops, SparseCore 0:
  10.2 87.5 all-gather.1

commit v2 on v1

--- a/solution.py
+++ b/solution.py
@@ -40,63 +40,80 @@
     pl.semaphore_wait(barrier, len(peers))
 
 
+def ring_order(m):
+    far = sorted(range(1, m), key=lambda d: (abs(2 * d - m), d))
+    return [(d, j) for j in range(4) for d in far], [(0, j) for j in range(1, 4)]
+
+
+def to_peer(me, m, d, j):
+    return lax.rem(me // 4 + d, m) * 4 + lax.rem(lax.rem(me, 4) + j, 4)
+
+
+def from_peer(me, m, d, j):
+    return lax.rem(me // 4 - d + m, m) * 4 + lax.rem(lax.rem(me, 4) - j + 4, 4)
+
+
 def dispatch_kernel(
     n, p, rows_ref, grads_ref, routed, cotan, local_sem, send, recv, relay_send, relay_recv
 ):
     me, t = lax.axis_index("sp"), lax.axis_index("tp")
-    width = rows_ref.shape[2]
-    others = [lax.rem(me + k, n) for k in range(1, n)]
+    m = n // 4
+    width = rows_ref.shape[2] // p
+    far, near = ring_order(m)
     sides = [lax.rem(t + k, p) for k in range(1, p)]
-    greet([(o, t) for o in others] + [(me, s) for s in sides])
+    greet([(to_peer(me, m, d, j), t) for d, j in far + near] + [(me, s) for s in sides])
     mine = pl.ds(pl.multiple_of(t * width, width), width)
     pairs = ((rows_ref, routed), (grads_ref, cotan))
+    sends = []
     started = []
     for a, (src, dst) in enumerate(pairs):
-        own = pltpu.make_async_copy(src.at[me], dst.at[me, :, mine], local_sem.at[a])
-        own.start()
-        started.append(own)
-    sends = []
-    for a, (src, dst) in enumerate(pairs):
-        for k in range(1, n):
-            to = others[k - 1]
+        for d, j in far:
+            to = to_peer(me, m, d, j)
+            i = d * 4 + j
             copy = remote(
-                src.at[to], dst.at[me, :, mine], send.at[a, k], recv.at[a, k], to, t
+                src.at[to, :, mine], dst.at[me, :, mine], send.at[a, i], recv.at[a, i], to, t
             )
             copy.start()
             sends.append(copy)
-        for j in range(1, p):
-            copy = remote(
-                src.at[me],
-                dst.at[me, :, mine],
-                relay_send.at[a, 0, j],
-                relay_recv.at[a, 0, j],
-                me,
-                sides[j - 1],
-            )
+        for d, j in near:
+            to = to_peer(me, m, d, j)
+            i = d * 4 + j
+            copy = remote(src.at[to], dst.at[me], send.at[a, i], recv.at[a, i], to, t)
             copy.start()
             sends.append(copy)
+        own = pltpu.make_async_copy(src.at[me], dst.at[me], local_sem.at[a])
+        own.start()
+        started.append(own)
     for a, (src, dst) in enumerate(pairs):
-        for k in range(1, n):
-            frm = lax.rem(me - k + n, n)
+        for d, j in far:
+            frm = from_peer(me, m, d, j)
+            i = d * 4 + j
             landed = dst.at[frm, :, mine]
-            remote(src.at[frm], landed, send.at[a, k], recv.at[a, k], frm, t).wait_recv()
-            for j in range(1, p):
+            remote(
+                src.at[frm, :, mine], landed, send.at[a, i], recv.at[a, i], frm, t
+            ).wait_recv()
+            for k in range(1, p):
                 copy = remote(
-                    landed, landed, relay_send.at[a, k, j], relay_recv.at[a, k, j], me, sides[j - 1]
+                    landed, landed, relay_send.at[a, i, k], relay_recv.at[a, i, k], me, sides[k - 1]
                 )
                 copy.start()
                 sends.append(copy)
     for own in started:
         own.wait()
     for a, (src, dst) in enumerate(pairs):
-        for k in range(n):
-            frm = lax.rem(me - k + n, n)
-            for j in range(1, p):
-                side = lax.rem(t - j + p, p)
+        for d, j in near:
+            frm = from_peer(me, m, d, j)
+            i = d * 4 + j
+            remote(src.at[frm], dst.at[frm], send.at[a, i], recv.at[a, i], frm, t).wait_recv()
+        for d, j in far:
+            frm = from_peer(me, m, d, j)
+            i = d * 4 + j
+            for k in range(1, p):
+                side = lax.rem(t - k + p, p)
                 theirs = pl.ds(pl.multiple_of(side * width, width), width)
                 landed = dst.at[frm, :, theirs]
                 remote(
-                    landed, landed, relay_send.at[a, k, j], relay_recv.at[a, k, j], me, side
+                    landed, landed, relay_send.at[a, i, k], relay_recv.at[a, i, k], me, side
                 ).wait_recv()
     for copy in sends:
         copy.wait_send()
@@ -104,7 +121,7 @@
 
 def dispatch(rows, grads, n, p):
     count, cap, width = rows.shape
-    out = jax.ShapeDtypeStruct((n, cap, width * p), BF16)
+    out = jax.ShapeDtypeStruct((n, cap, width), BF16)
     return pl.pallas_call(
         functools.partial(dispatch_kernel, n, p),
         out_shape=(out, out),
@@ -126,6 +143,7 @@
 def return_kernel(
     n,
     p,
+    cuts,
     part,
     pick,
     full,
@@ -141,59 +159,91 @@
     row_recv,
 ):
     me, t = lax.axis_index("sp"), lax.axis_index("tp")
-    width = stage.shape[2]
-    others = [lax.rem(me + k, n) for k in range(1, n)]
+    m = n // 4
+    width = full.shape[1] // p
+    span = width // cuts
+    far, near = ring_order(m)
+    every = far + near + [(0, 0)]
     sides = [lax.rem(t + k, p) for k in range(1, p)]
-    greet([(o, t) for o in others] + [(me, s) for s in sides])
+    greet([(to_peer(me, m, d, j), t) for d, j in far + near] + [(me, s) for s in sides])
+
+    def columns(side, q):
+        return pl.ds(pl.multiple_of(side * width + q * span, span), span)
+
     sends = []
-    for k in list(range(1, n)) + [0]:
-        to = lax.rem(me + k, n)
-        for j in range(1, p):
-            side = sides[j - 1]
-            theirs = pl.ds(pl.multiple_of(side * width, width), width)
-            copy = remote(
-                part.at[to, :, theirs],
-                beside.at[k, j],
-                side_send.at[k, j],
-                side_recv.at[k, j],
+    for q in range(cuts):
+        for d, j in every:
+            to = to_peer(me, m, d, j)
+            i = d * 4 + j
+            for k in range(1, p):
+                side = sides[k - 1]
+                copy = remote(
+                    part.at[to, :, columns(side, q)],
+                    beside.at[q, i, k],
+                    side_send.at[q, i, k],
+                    side_recv.at[q, i, k],
+                    me,
+                    side,
+                )
+                copy.start()
+                sends.append(copy)
+    def add_and_send(q, d, j):
+        mine = columns(t, q)
+        to = to_peer(me, m, d, j)
+        i = d * 4 + j
+        value = part[to, :, mine].astype(F32)
+        for k in range(1, p):
+            side = lax.rem(t - k + p, p)
+            remote(
+                part.at[to, :, mine],
+                beside.at[q, i, k],
+                side_send.at[q, i, k],
+                side_recv.at[q, i, k],
                 me,
                 side,
-            )
+            ).wait_recv()
+            value = value + beside[q, i, k].astype(F32)
+        stage[q, i] = value.astype(BF16)
+        if i > 0:
+            copy = remote(stage.at[q, i], back.at[q, i], send.at[q, i], recv.at[q, i], to, t)
             copy.start()
             sends.append(copy)
-    mine = pl.ds(pl.multiple_of(t * width, width), width)
-    for k in list(range(1, n)) + [0]:
-        to = lax.rem(me + k, n)
-        value = part[to, :, mine].astype(F32)
-        for j in range(1, p):
-            side = lax.rem(t - j + p, p)
+
+    def take(q, d, j):
+        frm = from_peer(me, m, d, j)
+        i = d * 4 + j
+        remote(stage.at[q, i], back.at[q, i], send.at[q, i], recv.at[q, i], frm, t).wait_recv()
+        total[...] += jnp.dot(pick[frm], back[q, i], preferred_element_type=F32)
+
+    for q in range(cuts + 1):
+        if q > 0:
+            total[...] = jnp.dot(pick[me], stage[q - 1, 0], preferred_element_type=F32)
+        for d, j in every:
+            if q < cuts:
+                add_and_send(q, d, j)
+            if q > 0 and d * 4 + j > 0:
+                take(q - 1, d, j)
+        if q > 0:
+            mine = columns(t, q - 1)
+            full[:, mine] = total[...].astype(BF16)
+            for k in range(1, p):
+                copy = remote(
+                    full.at[:, mine],
+                    full.at[:, mine],
+                    row_send.at[q - 1, k],
+                    row_recv.at[q - 1, k],
+                    me,
+                    sides[k - 1],
+                )
+                copy.start()
+                sends.append(copy)
+    for q in range(cuts):
+        for k in range(1, p):
+            side = lax.rem(t - k + p, p)
+            theirs = columns(side, q)
             remote(
-                part.at[to, :, mine], beside.at[k, j], side_send.at[k, j], side_recv.at[k, j], me, side
+                full.at[:, theirs], full.at[:, theirs], row_send.at[q, k], row_recv.at[q, k], me, side
             ).wait_recv()
-            value = value + beside[k, j].astype(F32)
-        stage[k] = value.astype(BF16)
-        if k > 0:
-            copy = remote(stage.at[k], back.at[k], send.at[k], recv.at[k], to, t)
-            copy.start()
-            sends.append(copy)
-    total[...] = jnp.dot(pick[me], stage[0], preferred_element_type=F32)
-    for k in range(1, n):
-        frm = lax.rem(me - k + n, n)
-        remote(stage.at[k], back.at[k], send.at[k], recv.at[k], frm, t).wait_recv()
-        total[...] += jnp.dot(pick[frm], back[k], preferred_element_type=F32)
-    full[:, mine] = total[...].astype(BF16)
-    for j in range(1, p):
-        copy = remote(
-            full.at[:, mine], full.at[:, mine], row_send.at[j], row_recv.at[j], me, sides[j - 1]
-        )
-        copy.start()
-        sends.append(copy)
-    for j in range(1, p):
-        side = lax.rem(t - j + p, p)
-        theirs = pl.ds(pl.multiple_of(side * width, width), width)
-        remote(
-            full.at[:, theirs], full.at[:, theirs], row_send.at[j], row_recv.at[j], me, side
-        ).wait_recv()
     for copy in sends:
         copy.wait_send()
 
@@ -202,22 +252,24 @@
     count, cap, whole = part.shape
     tokens = pick.shape[1]
     width = whole // p
+    cuts = 2 if width % 256 == 0 else 1
+    span = width // cuts
     return pl.pallas_call(
-        functools.partial(return_kernel, n, p),
+        functools.partial(return_kernel, n, p, cuts),
         out_shape=jax.ShapeDtypeStruct((tokens, whole), BF16),
         in_specs=[VMEM_SPEC] * 2,
         out_specs=VMEM_SPEC,
         scratch_shapes=[
-            pltpu.VMEM((n, p, cap, width), BF16),
-            pltpu.VMEM((n, cap, width), BF16),
-            pltpu.VMEM((n, cap, width), BF16),
-            pltpu.VMEM((tokens, width), F32),
-            pltpu.SemaphoreType.DMA((n, p)),
-            pltpu.SemaphoreType.DMA((n, p)),
-            pltpu.SemaphoreType.DMA((n,)),
-            pltpu.SemaphoreType.DMA((n,)),
-            pltpu.SemaphoreType.DMA((p,)),
-            pltpu.SemaphoreType.DMA((p,)),
+            pltpu.VMEM((cuts, n, p, cap, span), BF16),
+            pltpu.VMEM((cuts, n, cap, span), BF16),
+            pltpu.VMEM((cuts, n, cap, span), BF16),
+            pltpu.VMEM((tokens, span), F32),
+            pltpu.SemaphoreType.DMA((cuts, n, p)),
+            pltpu.SemaphoreType.DMA((cuts, n, p)),
+            pltpu.SemaphoreType.DMA((cuts, n)),
+            pltpu.SemaphoreType.DMA((cuts, n)),
+            pltpu.SemaphoreType.DMA((cuts, p)),
+            pltpu.SemaphoreType.DMA((cuts, p)),
         ],
         compiler_params=pltpu.CompilerParams(
             collective_id=1, has_side_effects=True, vmem_limit_bytes=VMEM_LIMIT
@@ -410,19 +462,17 @@
         for k in range(top_count)
     )
     select = taken.astype(BF16)
-    column_start = lax.axis_index("tp") * width_dev
-    part_rows = lax.dynamic_slice_in_dim(moe_input, column_start, width_dev, 1)
-    part_grads = lax.dynamic_slice_in_dim(out_grad, column_start, width_dev, 1)
-    send_rows = jnp.dot(select, part_rows, preferred_element_type=F32).astype(BF16)
+    send_rows = jnp.dot(select, moe_input, preferred_element_type=F32).astype(BF16)
     send_grads = (
-        slot_weight[:, None] * jnp.dot(select, part_grads, preferred_element_type=F32)
+        slot_weight[:, None] * jnp.dot(select, out_grad, preferred_element_type=F32)
     ).astype(BF16)
     routed, cotan = dispatch(
-        send_rows.reshape(experts, capacity, width_dev),
-        send_grads.reshape(experts, capacity, width_dev),
+        send_rows.reshape(experts, capacity, width),
+        send_grads.reshape(experts, capacity, width),
         n,
         p,
     )
+    routed, cotan, out_proj = lax.optimization_barrier((routed, cotan, out_proj))
     routed = routed.reshape(slots, width)
     cotan = cotan.reshape(slots, width)
     gate_w, lin_w, down_w = gate_weight[0], lin_weight[0], down_weight[0]

time: 268 us -> 241 us (0.90)
  Pallas kernels: 203 us -> 177 us
    pallas_call x1, Pallas kernels: 97.4 us -> 81.7 us  [dispatch(): pl.pallas_call(functools.partial(dispatch_kernel, n, p), out_shape=(out,...]
    pallas_call x1, Pallas kernels: 41.2 us -> 35.8 us  [scatter_sum(): pl.pallas_call(functools.partial(scatter_kernel, m, chunks), out_shape=ja...]
    pallas_call x1, Pallas kernels: 64.5 us -> 59.2 us  [return_rows(): pl.pallas_call(functools.partial(return_kernel, n, p, cuts), out_shape=ja...]
  transfers between devices with their start and end apart: 3 -> 3, of which waited for: 0 -> 0; matrix products, arithmetic and copies ran while one was open for 13% -> 11% of each run, Pallas kernels for 76% -> 40%
where the time goes in v2:
time: 241 us; the launch traced here: 240 us
  Pallas kernels  177 us (73%)
  matrix products  35.5 us (15%)
  between operations  14.3 us (6%)
  other arithmetic  7.25 us (3%)
  local copies, waits for them, and re-layouts  3.82 us (2%)
  starting transfers between devices  2.8 us (1%)
    pallas_call x1, Pallas kernels, dispatch(): pl.pallas_call(functools.partial(dispatch_kernel, n, p), out_shape=(out,...  81.7 us
    pallas_call x1, Pallas kernels, return_rows(): pl.pallas_call(functools.partial(return_kernel, n, p, cuts), out_shape=ja...  59.2 us
    pallas_call x1, Pallas kernels, scatter_sum(): pl.pallas_call(functools.partial(scatter_kernel, m, chunks), out_shape=ja...  35.8 us
    dot_general x10, matrix products, product(): lax.dot_general(a, b, (((left,), (right,)), ((), ())), preferred_element_...  29.4 us
  transfers between devices with their start and end apart: 3, of which 0 were waited for; matrix products, arithmetic and copies ran while one was open for 11% of the time, Pallas kernels for 40%

profile of v2, /device:TPU:0, one launch (start us, length us, event | category | flops | bytes accessed | tf_op | source)
XLA Modules:
  0.0 240.3 jit_solution(14072057411612043737)
XLA Ops:
  7.2 0.0 copy-start
  7.2 0.0 all-gather.2.cloned.1.call-start
  7.2 0.9 copy.28
  8.2 0.1 eq.71
  8.3 0.0 copy-start.3
  8.3 0.3 fusion.24
  8.6 0.1 convert_element_type.89
  8.8 0.1 copy.29
  8.8 0.7 multiply_add_fusion.1
  9.5 0.8 fusion.57
  10.3 3.6 %convolution_convert_fusion.1 = bf16[640,2048]{1,0:T(8,128)(2,1)} fusion(bf16[256,2048]{1,0:T(8,128)(2,1)} %param.12, s32[256]{0:T(256)S(1)} %bitcast.104, s32[256]{0:T(256)S(1)} %bitcast.100), kind=kOutput, calls=%fused_computation.3 | convolution fusion | flops 672890880 | bytes 3672064 | tf_op jit(solution)/shard_map/dot_general | solution.py:465
  13.9 0.2 select_reduce_fusion
  14.1 2.3 multiply_convert_fusion
  16.5 81.7 %shard_map.171 = (bf16[16,40,2048]{2,1,0:T(8,128)(2,1)}, bf16[16,40,2048]{2,1,0:T(8,128)(2,1)}) custom-call(bf16[16,40,2048]{2,1,0:T(8,128)(2,1)} %bitcast.97, bf16[16,40,2048]{2,1,0:T(8,128)(2,1)} %bitcast.99), custom_call_target="tpu_custom_call" | custom-call | tf_op jit(solution)/shard_map/pallas_call | solution.py:125
  98.2 0.0 all-gather.2.cloned.1.call-update
  98.2 1.5 fusion.28
  99.8 1.5 collective-permute-start
  101.3 1.3 or_convert_fusion.pick
  102.6 0.0 copy-done
  102.6 1.6 fusion.10
  104.2 0.0 copy-done.11
  104.2 0.0 copy-start.9
  104.3 0.0 copy-start.10
  104.3 1.6 fusion.4
  105.8 0.2 copy-done.9
  106.0 0.6 copy-done.10
  106.6 2.3 fusion.17
  108.9 3.2 %fusion.1 = bf16[1,512,2048]{2,1,0:T(8,128)(2,1)} fusion(bf16[512,640]{0,1:T(8,128)(2,1)S(1)} %get-tuple-element.21, bf16[640,2048]{1,0:T(8,128)(2,1)S(1)} %bitcast.95), kind=kOutput, calls=%fused_computation.8 | convolution fusion | flops 1343225856 | bytes 5373952 | tf_op jit(solution)/shard_map/dot_general | solution.py:481
  112.1 3.2 %fusion = bf16[1,512,2048]{2,1,0:T(8,128)(2,1)} fusion(bf16[512,640]{0,1:T(8,128)(2,1)S(1)} %get-tuple-element.22, bf16[640,2048]{1,0:T(8,128)(2,1)S(1)} %bitcast.96), kind=kOutput, calls=%fused_computation.7 | convolution fusion | flops 1343225856 | bytes 5373952 | tf_op jit(solution)/shard_map/dot_general | solution.py:481
  115.3 1.6 fusion.8
  116.8 3.0 %add_convert_fusion = bf16[640,2048]{1,0:T(8,128)(2,1)} fusion(f32[640,2048]{1,0:T(8,128)S(1)} %fusion.8, bf16[512,640]{0,1:T(8,128)(2,1)S(1)} %get-tuple-element.21, bf16[1,512,2048]{2,1,0:T(8,128)(2,1)S(1)} %copy-done.11), kind=kOutput, calls=%fused_computation | convolution fusion | flops 1344798720 | bytes 10616832 | tf_op jit(solution)/shard_map/dot_general | solution.py:481
  119.9 3.6 %fusion.2 = bf16[1,512,2048]{2,1,0:T(8,128)(2,1)} fusion(bf16[640,2048]{1,0:T(8,128)(2,1)S(1)} %bitcast.117, f32[640,512]{1,0:T(8,128)S(1)} %fusion.10, f32[640,512]{1,0:T(8,128)S(1)} %fusion.4), kind=kOutput, calls=%fused_computation.9 | convolution fusion | flops 1346502656 | bytes 7340032 | tf_op jit(solution)/shard_map/dot_general | solution.py:481
  123.5 59.2 %shard_map.172 = bf16[256,2048]{1,0:T(8,128)(2,1)} custom-call(bf16[16,40,2048]{2,1,0:T(8,128)(2,1)} %bitcast.98, bf16[16,256,40]{2,1,0:T(8,128)(2,1)} %or_convert_fusion.pick), custom_call_target="tpu_custom_call" | custom-call | tf_op jit(solution)/shard_map/pallas_call | solution.py:257
  182.7 0.0 collective-permute-done
  182.7 1.1 maximum_convert_fusion
  183.8 6.0 %multiply_convert_fusion.1 = (bf16[256,1024]{1,0:T(8,128)(2,1)}, f32[256,1024]{1,0:T(8,128)S(1)}, bf16[256,1024]{1,0:T(8,128)(2,1)S(1)}) fusion(f32[258,1024]{1,0:T(8,128)} %maximum_convert_fusion, f32[1024]{0:T(1024)S(1)} %bitcast.110, f32[1024]{0:T(1024)S(1)} %bitcast.112, f32[1024]{0:T(1024)S(1)} %bitcast.108, bf16[256,1024]{1,0:T(8,128)(2,1)} %param.19, ...), kind=kOutput, calls=%fused_computation.60 | convolution fusion | flops 1078460416 | bytes 12070912 | tf_op jit(solution)/shard_map/dot_general | solution.py:481
  189.8 1.3 collective-permute-start.1
  191.1 0.0 copy-done.2
  191.2 0.0 copy-done.7
  191.2 3.3 %convolution_convert_fusion = bf16[2048,1024]{1,0:T(8,128)(2,1)} fusion(f32[256,1024]{1,0:T(8,128)S(1)} %get-tuple-element.20, bf16[256,1024]{1,0:T(8,128)(2,1)S(1)} %copy-done.7, bf16[256,2048]{1,0:T(8,128)(2,1)S(1)} %copy-done.2, bf16[256,2048]{1,0:T(8,128)(2,1)S(1)} %copy-done.3), kind=kOutput, calls=%fused_computation.2 | convolution fusion | flops 1078722560 | bytes 7864320 | tf_op jit(solution)/shard_map/dot_general | solution.py:481
  194.5 35.8 %shard_map.173 = f32[128,1024]{1,0:T(8,128)} custom-call(bf16[4,2,2,128,1024]{4,3,2,1,0:T(8,128)(2,1)} %bitcast.92), custom_call_target="tpu_custom_call" | custom-call | tf_op jit(solution)/shard_map/pallas_call | solution.py:396
  230.3 0.0 collective-permute-done.1
  230.3 0.1 maximum_convert_fusion.1
  230.4 0.0 copy-start.6
  230.4 1.2 fusion.27
  231.6 1.0 fusion.29
  232.6 0.1 copy-done.5
  232.7 0.8 copy.32
  (20 shorter events, 0.1 us)
Async XLA Ops:
  7.2 95.4 %copy-start = (bf16[1,512,2048]{2,1,0:T(8,128)(2,1)S(1)}, bf16[1,512,2048]{2,1,0:T(8,128)(2,1)}, u32[]{:S(2)}) copy-start(bf16[1,512,2048]{2,1,0:T(8,128)(2,1)} %param.16) | copy-start | bytes 6291460
  7.2 176.6 %all-gather.2.cloned.1.call-start = ((), (), s32[]{:S(2)}) async-start(), calls=%async_computation | async-start | bytes 4456448 | tf_op jit(solution)/shard_map/all_gather | solution.py:516
  8.3 5.8 %copy-start.3 = (bf16[256,2048]{1,0:T(8,128)(2,1)S(1)}, bf16[256,2048]{1,0:T(8,128)(2,1)}, u32[]{:S(2)}) copy-start(bf16[256,2048]{1,0:T(8,128)(2,1)} %param.13) | copy-start | bytes 3145732
  98.2 4.4 %copy-start.1 = (bf16[16,40,2048]{2,1,0:T(8,128)(2,1)S(1)}, bf16[16,40,2048]{2,1,0:T(8,128)(2,1)}, u32[]{:S(2)}) copy-start(bf16[16,40,2048]{2,1,0:T(8,128)(2,1)} %get-tuple-element.14) | copy-start | bytes 7864324
  99.8 82.9 %collective-permute-start = (bf16[2,1024]{1,0:T(2,128)(2,1)S(1)}, bf16[2,1024]{1,0:T(2,128)(2,1)S(1)}, u32[]{:S(2)}, u32[]{:S(2)}) collective-permute-start(bf16[2,1024]{1,0:T(2,128)(2,1)S(1)} %slice.67), channel_id=1, source_target_pairs={{0,2},{2,4},{4,6},{6,8},{8,10},{10,12},{12,14},{14,16},{16,18},{18... | collective-permute-start | bytes 12296 | tf_op jit(solution)/shard_map/ppermute | solution.py:22
  102.6 1.6 copy-start.11
  104.2 1.7 copy-start.9
  104.3 2.4 copy-start.10
  119.9 3.6 %copy-start.8 = (f32[3,1024]{1,0:T(4,128)S(1)}, f32[3,1024]{1,0:T(4,128)}, u32[]{:S(2)}) copy-start(f32[3,1024]{1,0:T(4,128)} %param.22) | copy-start | bytes 36868
  183.8 7.3 %copy-start.2 = (bf16[256,2048]{1,0:T(8,128)(2,1)S(1)}, bf16[256,2048]{1,0:T(8,128)(2,1)}, u32[]{:S(2)}) copy-start(bf16[256,2048]{1,0:T(8,128)(2,1)} %shard_map.172) | copy-start | bytes 3145732
  183.8 7.3 %copy-start.7 = (bf16[256,1024]{1,0:T(8,128)(2,1)S(1)}, bf16[256,1024]{1,0:T(8,128)(2,1)}, u32[]{:S(2)}) copy-start(bf16[256,1024]{1,0:T(8,128)(2,1)} %param.19) | copy-start | bytes 1572868
  189.8 40.5 %collective-permute-start.1 = (bf16[2,1024]{1,0:T(2,128)(2,1)S(1)}, bf16[2,1024]{1,0:T(2,128)(2,1)S(1)}, u32[]{:S(2)}, u32[]{:S(2)}) collective-permute-start(bf16[2,1024]{1,0:T(2,128)(2,1)S(1)} %slice.71), channel_id=1, source_target_pairs={{2,0},{4,2},{6,4},{8,6},{10,8},{12,10},{14,12},{16,14},{18,16},{20... | collective-permute-start | bytes 12296 | tf_op jit(solution)/shard_map/ppermute | solution.py:22
  194.5 35.9 %copy-start.4 = (bf16[256,1024]{1,0:T(8,128)(2,1)S(1)}, bf16[256,1024]{1,0:T(8,128)(2,1)}, u32[]{:S(2)}) copy-start(bf16[256,1024]{1,0:T(8,128)(2,1)} %param.20) | copy-start | bytes 1572868
  230.4 1.2 copy-start.6
  231.6 1.0 copy-start.5
Sparse Core Ops, SparseCore 0:
  98.3 66.4 all-gather.1
